TPU v7x, 32 devices: a whole 2x2x4 slice. The times are simulated.
32 devices in a mesh: ep: 4 (over y, x), tp: 8 (over z, core).
Axes of the slice: x: 2, y: 2, z: 4, core: 2. Of those that a mesh axis runs over, the one named last changes fastest.
Arguments:
- tokens: bfloat16 [128, 4096], P('ep', 'tp'), may hold values from -16 to 16
- routing: int32 [128, 4], P('ep'), may hold values from 0 to 7, all different within a row; in each aligned block of 32 rows (0 to 31, 32 to 63, ...) at most 32 rows name the same one
- gate_weights: float32 [128, 4], P('ep'), may hold values from 0.1 to 1
- w_gate: bfloat16 [8, 1024, 4096], P('ep', 'tp'), may hold values from -0.09375 to 0.09375
- w_up: bfloat16 [8, 1024, 4096], P('ep', 'tp'), may hold values from -0.09375 to 0.09375
- w_down: bfloat16 [8, 1024, 4096], P('ep', None, 'tp'), may hold values from -2 to 2
- out_gain: float32 [4096], P('tp'), may hold values from 0.1 to 1.9
Outputs:
- mixed: bfloat16 [128, 4096], P('ep', 'tp')
Inputs may be any that keep to these rules, and one draw needn't show every extreme that they name: `routing`: in each aligned block of 32 rows (the tokens of one index of ep) no expert is named by more than 32 entries, and in every draw some expert is named by exactly 32 entries of some block. The 4 entries of a row differ.
All inputs are finite; a program needn't handle non-finite values.
Results may differ from a plain program's by a relative error of at most 0.0057.
Values may be sent and summed in bfloat16 or wider, within the bound.
A program may use at most 64 MiB of HBM per device.

v0:
```python
import jax
import jax.numpy as jnp
from jax import lax
from jax.sharding import PartitionSpec as P

D = 4096
TOPK = 4
EXP_DEV = 2


norm_eps = 1e-05


def body(tokens, routing, gate_weights, w_gate, w_up, w_down, out_gain):
    ep_count = lax.axis_size("ep")
    tok_rows = tokens.shape[0]
    width_part = tokens.shape[1]
    experts = EXP_DEV * ep_count
    slot_count = 2 * tok_rows * TOPK // experts
    span_rows = ep_count * slot_count
    total_slots = EXP_DEV * span_rows
    flat_route = routing.reshape(-1)
    expert_ids = jnp.arange(experts, dtype=jnp.int32)
    hit_table = (flat_route[:, None] == expert_ids[None, :]).astype(jnp.int32)
    running = jnp.cumsum(hit_table, axis=0) - hit_table
    slot_rank = jnp.sum(running * hit_table, axis=1)
    slot_target = flat_route % EXP_DEV * span_rows + flat_route // EXP_DEV * slot_count + slot_rank
    entry_targets = slot_target.reshape(tok_rows, TOPK)
    slot_ids = jnp.arange(total_slots, dtype=jnp.int32)
    select_table = jnp.any(entry_targets[None, :, :] == slot_ids[:, None, None], axis=2).astype(
        jnp.bfloat16
    )
    outgoing = jnp.dot(select_table, tokens, preferred_element_type=jnp.float32).astype(
        jnp.bfloat16
    )
    outgoing = outgoing.reshape(EXP_DEV, ep_count, slot_count, width_part)
    arrived = lax.all_to_all(outgoing, "ep", split_axis=1, concat_axis=1, tiled=True).reshape(
        EXP_DEV, span_rows, width_part
    )
    piece_cols = lax.all_gather(arrived, "tp", axis=2, tiled=True)
    gate_sum = jnp.einsum("efn,esn->efs", w_gate, piece_cols, preferred_element_type=jnp.float32)
    up_sum = jnp.einsum("efn,esn->efs", w_up, piece_cols, preferred_element_type=jnp.float32)
    square_sum = jnp.einsum(
        "esn,esn->es", piece_cols, piece_cols, preferred_element_type=jnp.float32
    )
    row_scale = lax.rsqrt(square_sum / D + norm_eps)[:, None, :]
    hidden = (jax.nn.silu(gate_sum * row_scale) * (up_sum * row_scale)).astype(jnp.bfloat16)
    out_part = w_down.shape[2]
    expert_out = jnp.einsum(
        "ens,end->esd",
        lax.all_gather(hidden, "tp", axis=1, tiled=True),
        w_down,
        preferred_element_type=jnp.float32,
    ).astype(jnp.bfloat16)
    returned = lax.all_to_all(
        expert_out.reshape(EXP_DEV, ep_count, slot_count, out_part),
        "ep",
        split_axis=1,
        concat_axis=1,
        tiled=True,
    )
    returned = returned.reshape(total_slots, out_part)
    chosen = returned[slot_target].astype(jnp.float32).reshape(tok_rows, TOPK, out_part)
    combined = jnp.sum(chosen * gate_weights[:, :, None], axis=1)
    square_total = lax.psum(jnp.sum(combined * combined, axis=1), "tp")
    final_scale = lax.rsqrt(square_total / D + norm_eps)
    return (combined * final_scale[:, None] * out_gain[None, :]).astype(jnp.bfloat16)


def solution(mesh):
    placed = (
        P("ep", "tp"),
        P("ep", None),
        P("ep", None),
        P("ep", "tp", None),
        P("ep", "tp", None),
        P("ep", None, "tp"),
        P("tp"),
    )
    return jax.shard_map(body, mesh=mesh, in_specs=placed, out_specs=P("ep", "tp"), check_vma=False)
```

profile of v0, /device:TPU:0, one launch (start us, length us, event | category | flops | bytes accessed | tf_op | source)
XLA Modules:
  0.0 102.4 jit_solution(12375172439346588443)
XLA Ops:
  6.5 0.9 copy.33
  7.5 0.1 eq.30
  7.7 0.2 reduce_window_sum.11
  7.8 0.2 select_reduce_fusion
  8.0 0.1 reduce_sum.32
  8.2 0.1 fusion.5
  8.3 1.0 convolution_convert_fusion
  9.4 10.7 %all_to_all.10 = bf16[2,4,32,512]{3,2,0,1:T(8,128)(2,1)S(1)} all-to-all(bf16[2,4,32,512]{3,2,0,1:T(8,128)(2,1)S(1)} %copy.39), channel_id=1, replica_groups=mesh['ep'=4,'tp'=8] {'ep'}, dimensions={1} | all-to-all | bytes 524288 | tf_op jit(solution)/shard_map/all_to_all | solution.py:37
  20.1 0.7 copy.40
  20.9 0.1 reshape.182
  21.0 28.9 %all-gather.2.cloned.1.call-done = bf16[2,128,4096]{2,1,0:T(8,128)(2,1)} async-done(((bf16[2,128,512]{2,1,0:T(8,128)(2,1)}), bf16[2,128,4096]{2,1,0:T(8,128)(2,1)}) %all-gather.2.cloned.1.call-update) | async-done | bytes 2097168 | tf_op jit(solution)/shard_map/all_gather | solution.py:40
  49.9 2.2 %fusion = f32[2,128]{1,0:T(2,128)S(1)} fusion(bf16[2,128,4096]{2,1,0:T(8,128)(2,1)} %all-gather.2.cloned.1.call-done), kind=kLoop, calls=%fused_computation.2 | loop fusion | flops 3145472 | bytes 2098176 | tf_op jit(solution)/shard_map/esn,esn->es/dot_general | solution.py:43
  52.2 2.5 %fusion.3 = f32[2,128,128]{1,2,0:T(8,128)S(1)} fusion(bf16[2,128,4096]{2,1,0:T(8,128)(2,1)S(1)} %copy-done.1, bf16[2,128,4096]{2,1,0:T(8,128)(2,1)} %param.10, f32[2,128]{1,0:T(2,128)S(1)} %add_rsqrt_fusion), kind=kOutput, calls=%fused_computation.9 | convolution fusion | flops 268468224 | bytes 4326400 | tf_op jit(solution)/shard_map/efn,esn->efs/dot_general | solution.py:41
  54.6 0.7 fusion.4
  55.3 13.9 %all_gather.7 = bf16[2,1024,128]{1,2,0:T(8,128)(2,1)S(1)} all-gather(bf16[2,128,128]{1,2,0:T(8,128)(2,1)S(1)} %fusion.4), channel_id=1, replica_groups=mesh['ep'=4,'tp'=8] {'tp'}, dimensions={1}, use_global_device_ids=true | all-gather | bytes 589824 | tf_op jit(solution)/shard_map/all_gather | solution.py:51
  69.2 0.4 convolution_convert_fusion.1
  69.7 0.7 copy.41
  70.4 3.6 %all-to-all-start.1 = ((bf16[2,4,32,512]{3,2,0,1:T(8,128)(2,1)}), bf16[2,4,32,512]{3,2,0,1:T(8,128)(2,1)S(1)}, u32[]{:S(2)}, u32[]{:S(2)}) async-start(bf16[2,4,32,512]{3,2,0,1:T(8,128)(2,1)} %copy.41), calls=%async_computation.1 | async-start | bytes 524288 | tf_op jit(solution)/shard_map/all_to_all | solution.py:55
  74.2 5.8 %all-to-all-done.1 = bf16[2,4,32,512]{3,2,0,1:T(8,128)(2,1)S(1)} async-done(((bf16[2,4,32,512]{3,2,0,1:T(8,128)(2,1)}), bf16[2,4,32,512]{3,2,0,1:T(8,128)(2,1)S(1)}, u32[]{:S(2)}, u32[]{:S(2)}) %all-to-all-start.1) | async-done | bytes 262176 | tf_op jit(solution)/shard_map/all_to_all | solution.py:55
  80.0 0.8 gather_fusion
  80.9 0.2 multiply_reduce_fusion
  81.1 0.1 multiply_reduce_fusion.1
  81.2 13.6 %psum.7 = f32[32]{0:T(128)S(1)} all-reduce(f32[32]{0:T(128)S(1)} %multiply_reduce_fusion.1), channel_id=1, replica_groups=mesh['ep'=4,'tp'=8] {'tp'}, use_global_device_ids=true, to_apply=%region_5.6 | all-reduce | flops 32 | bytes 256 | tf_op jit(solution)/shard_map/psum | solution.py:65
  94.8 0.7 multiply_convert_fusion
  (23 shorter events, 0.5 us)
Async XLA Ops:
  6.5 62.7 %copy-start = (bf16[2,1024,512]{2,1,0:T(8,128)(2,1)S(1)}, bf16[2,1024,512]{2,1,0:T(8,128)(2,1)}, u32[]{:S(2)}) copy-start(bf16[2,1024,512]{2,1,0:T(8,128)(2,1)} %param.12) | copy-start | bytes 6291460
  6.5 43.4 %all-gather.2.cloned.1.call-start = ((), (), s32[]{:S(2)}) async-start(), calls=%async_computation.2 | async-start | bytes 2359296 | tf_op jit(solution)/shard_map/all_gather | solution.py:40
  49.9 2.2 %copy-start.1 = (bf16[2,128,4096]{2,1,0:T(8,128)(2,1)S(1)}, bf16[2,128,4096]{2,1,0:T(8,128)(2,1)}, u32[]{:S(2)}) copy-start(bf16[2,128,4096]{2,1,0:T(8,128)(2,1)} %all-gather.2.cloned.1.call-done) | copy-start | bytes 6291460
  52.1 2.5 %copy-start.4 = (bf16[2,128,4096]{2,1,0:T(8,128)(2,1)S(1)}, bf16[2,128,4096]{2,1,0:T(8,128)(2,1)}, u32[]{:S(2)}) copy-start(bf16[2,128,4096]{2,1,0:T(8,128)(2,1)} %param.11) | copy-start | bytes 6291460
  69.2 4.8 %copy-start.2 = (f32[32,4]{0,1:T(4,128)S(1)}, f32[32,4]{0,1:T(4,128)}, u32[]{:S(2)}) copy-start(f32[32,4]{0,1:T(4,128)} %param.9) | copy-start | bytes 1540
  69.7 25.2 %copy-start.3 = (f32[512]{0:T(512)S(1)}, f32[512]{0:T(512)}, u32[]{:S(2)}) copy-start(f32[512]{0:T(512)} %param.13) | copy-start | bytes 6148
  70.4 9.5 %all-to-all-start.1 = ((bf16[2,4,32,512]{3,2,0,1:T(8,128)(2,1)}), bf16[2,4,32,512]{3,2,0,1:T(8,128)(2,1)S(1)}, u32[]{:S(2)}, u32[]{:S(2)}) async-start(bf16[2,4,32,512]{3,2,0,1:T(8,128)(2,1)} %copy.41), calls=%async_computation.1 | async-start | bytes 524288 | tf_op jit(solution)/shard_map/all_to_all | solution.py:55
Sparse Core Ops, SparseCore 0:
  21.0 28.8 all-gather.1
where the time goes:
time: 103 us; the launch traced here: 102 us
  blocking collectives  38.2 us (37%)
  waiting for transfers between devices  34.7 us (34%)
  between operations  13.5 us (13%)
  matrix products  4.63 us (4%)
  other arithmetic  3.86 us (4%)
  local copies, waits for them, and re-layouts  3.84 us (4%)
  starting transfers between devices  3.65 us (4%)
    all_gather x1, waiting for transfers between devices, body(): piece_cols = lax.all_gather(arrived, 'tp', axis=2, tiled=True)  28.9 us
    all_gather x1, blocking collectives, body(): lax.all_gather(hidden, 'tp', axis=1, tiled=True)  13.9 us
    psum x1, blocking collectives, body(): square_total = lax.psum(jnp.sum(combined * combined, axis=1), 'tp')  13.6 us
    all_to_all x1, blocking collectives, body(): lax.all_to_all(outgoing, 'ep', split_axis=1, concat_axis=1, tiled=True)  10.7 us
    all_to_all x1, waiting for transfers between devices, body(): lax.all_to_all(expert_out.reshape(EXP_DEV, ep_count, slot_count, out_part...  5.77 us
    all_to_all x1, starting transfers between devices, body(): lax.all_to_all(expert_out.reshape(EXP_DEV, ep_count, slot_count, out_part...  3.65 us
    dot_general x1, matrix products, body(): jnp.einsum('efn,esn->efs', w_gate, piece_cols, preferred_element_type=jnp...  2.45 us
    dot_general x1, other arithmetic, body(): jnp.einsum('esn,esn->es', piece_cols, piece_cols, preferred_element_type=...  2.23 us
  transfers between devices with their start and end apart: 2, of which 2 were waited for; matrix products, arithmetic and copies ran while one was open for 0% of the time, Pallas kernels for 0%

commit v1 on v0

--- a/solution.py
+++ b/solution.py
@@ -1,6 +1,10 @@
+import functools
+
 import jax
 import jax.numpy as jnp
 from jax import lax
+from jax.experimental import pallas as pl
+from jax.experimental.pallas import tpu as pltpu
 from jax.sharding import PartitionSpec as P
 
 D = 4096
@@ -11,7 +15,7 @@
 norm_eps = 1e-05
 
 
-def body(tokens, routing, gate_weights, w_gate, w_up, w_down, out_gain):
+def routed_body(tokens, routing, gate_weights, w_gate, w_up, w_down, out_gain):
     ep_count = lax.axis_size("ep")
     tok_rows = tokens.shape[0]
     width_part = tokens.shape[1]
@@ -67,6 +71,280 @@
     return (combined * final_scale[:, None] * out_gain[None, :]).astype(jnp.bfloat16)
 
 
+MESH = pl.DeviceIdType.MESH
+CORES = 2
+LANES = 128
+
+
+def dense_kernel(
+    n_ep,
+    n_tp,
+    tok_hbm,
+    route_ref,
+    gates_ref,
+    wg_hbm,
+    wu_hbm,
+    wd_hbm,
+    gain_ref,
+    out_ref,
+    x_all,
+    g_all,
+    w_v,
+    wd_v,
+    acc,
+    h_all,
+    p_send,
+    p_recv,
+    s_send,
+    s_all,
+    loc_sem,
+    snd_sem,
+    x_sem,
+    g_sem,
+    h_sem,
+    p_sem,
+    s_sem,
+):
+    e = lax.axis_index("ep")
+    t = lax.axis_index("tp")
+    n_z = n_tp // CORES
+    z = t // CORES
+    c = t % CORES
+    mate = z * CORES + (1 - c)
+    rows, width = tok_hbm.shape
+    tokens = rows * n_ep
+    n_exp, hid = wg_hbm.shape[0], wg_hbm.shape[1]
+    features = wg_hbm.shape[2]
+    mine = pl.ds(pl.multiple_of(e * rows, rows), rows)
+
+    barrier = pltpu.get_barrier_semaphore()
+    tp_peers = [lax.rem(t + d, n_tp) for d in range(1, n_tp)]
+    ep_peers = [lax.rem(e + d, n_ep) for d in range(1, n_ep)]
+    z_order = [0]
+    for d in range(1, n_z // 2 + 1):
+        z_order += [d] if 2 * d == n_z else [d, n_z - d]
+    z_list = [lax.rem(z + d, n_z) for d in z_order]
+    for peer in tp_peers:
+        pl.semaphore_signal(barrier, inc=1, device_id=(e, peer), device_id_type=MESH)
+    for peer in ep_peers:
+        pl.semaphore_signal(barrier, inc=1, device_id=(peer, t), device_id_type=MESH)
+
+    tok_copy = pltpu.make_async_copy(tok_hbm, x_all.at[t, mine, :], loc_sem.at[0])
+    tok_copy.start()
+    wg_copy = pltpu.make_async_copy(wg_hbm, w_v.at[0:n_exp], loc_sem.at[1])
+    wg_copy.start()
+    wu_copy = pltpu.make_async_copy(wu_hbm, w_v.at[n_exp : 2 * n_exp], loc_sem.at[2])
+    wu_copy.start()
+    wd_copy = pltpu.make_async_copy(wd_hbm, wd_v, loc_sem.at[3])
+    wd_copy.start()
+
+    lane = lax.broadcasted_iota(jnp.int32, (rows, LANES), 1)
+    table = jnp.zeros((rows, LANES), jnp.float32)
+    for k in range(route_ref.shape[1]):
+        table += jnp.where(route_ref[:, k : k + 1] == lane, gates_ref[:, k : k + 1], 0.0)
+    g_all[mine, :] = table
+
+    sends = []
+
+    def send(src, dst, recv, device):
+        copy = pltpu.make_async_remote_copy(
+            src_ref=src,
+            dst_ref=dst,
+            send_sem=snd_sem.at[len(sends)],
+            recv_sem=recv,
+            device_id=device,
+            device_id_type=MESH,
+        )
+        copy.start()
+        sends.append(copy)
+
+    def arrive(dst, recv):
+        pltpu.make_async_remote_copy(
+            src_ref=dst,
+            dst_ref=dst,
+            send_sem=snd_sem.at[0],
+            recv_sem=recv,
+            device_id=(e, mate),
+            device_id_type=MESH,
+        ).wait_recv()
+
+    def x_block(ep, tp):
+        return x_all.at[tp, pl.ds(pl.multiple_of(ep * rows, rows), rows), :]
+
+    def send_x(ep, tp, device):
+        send(x_block(ep, tp), x_block(ep, tp), x_sem.at[ep, tp], device)
+
+    tok_copy.wait()
+    pl.semaphore_wait(barrier, n_tp - 1 + n_ep - 1)
+
+    for zz in z_list[1:]:
+        send_x(e, t, (e, zz * CORES + c))
+    for peer in ep_peers:
+        send_x(e, t, (peer, t))
+    send_x(e, t, (e, mate))
+    for peer in ep_peers:
+        send(g_all.at[mine, :], g_all.at[mine, :], g_sem.at[e], (peer, t))
+    for zz in z_list[1:]:
+        tp = zz * CORES + c
+        arrive(x_block(e, tp), x_sem.at[e, tp])
+        for peer in ep_peers:
+            send_x(e, tp, (peer, t))
+        send_x(e, tp, (e, mate))
+    wg_copy.wait()
+    wu_copy.wait()
+
+    square = jnp.zeros((tokens, LANES), jnp.float32)
+
+    def up_part(tp, first, square):
+        x = x_all[tp]
+        cols = pl.ds(pl.multiple_of(tp * width, width), width)
+        w = w_v[:, :, cols].reshape(2 * n_exp * hid, width)
+        part = lax.dot_general(
+            x, w, (((1,), (1,)), ((), ())), preferred_element_type=jnp.float32
+        )
+        if first:
+            acc[...] = part
+        else:
+            acc[...] += part
+        for i in range(width // LANES):
+            piece = x[:, i * LANES : (i + 1) * LANES].astype(jnp.float32)
+            square = square + piece * piece
+        return square
+
+    for i, zz in enumerate(z_list):
+        tp = zz * CORES + c
+        for peer in ep_peers:
+            arrive(x_block(peer, tp), x_sem.at[peer, tp])
+            send_x(peer, tp, (e, mate))
+        square = up_part(tp, i == 0, square)
+    for zz in z_list:
+        tp = zz * CORES + 1 - c
+        for ep in [e] + ep_peers:
+            arrive(x_block(ep, tp), x_sem.at[ep, tp])
+        square = up_part(tp, False, square)
+    for peer in ep_peers:
+        theirs = g_all.at[pl.ds(pl.multiple_of(peer * rows, rows), rows), :]
+        arrive(theirs, g_sem.at[peer])
+
+    scale = lax.rsqrt(jnp.sum(square, axis=1, keepdims=True) / features + norm_eps)
+    every_lane = lax.broadcasted_iota(jnp.int32, (tokens, LANES), 1)
+    for j in range(n_exp):
+        gate = acc[:, j * hid : (j + 1) * hid] * scale
+        up = acc[:, (n_exp + j) * hid : (n_exp + j + 1) * hid] * scale
+        weight = jnp.sum(
+            jnp.where(every_lane == e * n_exp + j, g_all[...], 0.0), axis=1, keepdims=True
+        )
+        h_all[t, :, j * hid : (j + 1) * hid] = (
+            gate / (1.0 + jnp.exp(-gate)) * up * weight
+        ).astype(jnp.bfloat16)
+
+    def send_h(tp, device):
+        send(h_all.at[tp], h_all.at[tp], h_sem.at[tp], device)
+
+    for zz in z_list[1:]:
+        send_h(t, (e, zz * CORES + c))
+    send_h(t, (e, mate))
+    wd_copy.wait()
+
+    def down_part(tp, first):
+        part = None
+        for j in range(n_exp):
+            units = pl.ds(pl.multiple_of(tp * hid, hid), hid)
+            one = jnp.dot(
+                h_all[tp, :, j * hid : (j + 1) * hid],
+                wd_v[j, units, :],
+                preferred_element_type=jnp.float32,
+            )
+            part = one if part is None else part + one
+        if first:
+            acc[...] = part
+        else:
+            acc[...] += part
+
+    down_part(t, True)
+    arrive(h_all.at[mate], h_sem.at[mate])
+    down_part(mate, False)
+    for zz in z_list[1:]:
+        tp = zz * CORES + c
+        arrive(h_all.at[tp], h_sem.at[tp])
+        send_h(tp, (e, mate))
+        down_part(tp, False)
+    for zz in z_list[1:]:
+        tp = zz * CORES + 1 - c
+        arrive(h_all.at[tp], h_sem.at[tp])
+        down_part(tp, False)
+
+    for peer in ep_peers:
+        theirs = pl.ds(pl.multiple_of(peer * rows, rows), rows)
+        p_send[peer] = acc[theirs, :].astype(jnp.bfloat16)
+        send(p_send.at[peer], p_recv.at[e], p_sem.at[e], (peer, t))
+    combined = acc[mine, :]
+    for peer in ep_peers:
+        arrive(p_recv.at[peer], p_sem.at[peer])
+        combined = combined + p_recv[peer].astype(jnp.float32)
+
+    column = jnp.sum(combined * combined, axis=1, keepdims=True)
+    eye = lax.broadcasted_iota(jnp.int32, (rows, LANES), 0) == lane
+    s_send[...] = jnp.sum(jnp.where(eye, column, 0.0), axis=0, keepdims=True)
+    for peer in tp_peers:
+        send(s_send, s_all.at[t], s_sem.at[t], (e, peer))
+    total = s_send[...]
+    for peer in tp_peers:
+        arrive(s_all.at[peer], s_sem.at[peer])
+        total = total + s_all[peer]
+    total = jnp.sum(jnp.where(eye, total, 0.0), axis=1, keepdims=True)
+    final = lax.rsqrt(total / features + norm_eps)
+    out_ref[...] = (combined * final * gain_ref[...]).astype(jnp.bfloat16)
+    for copy in sends:
+        copy.wait_send()
+
+
+def dense_body(tokens, routing, gate_weights, w_gate, w_up, w_down, out_gain):
+    n_ep, n_tp = lax.axis_size("ep"), lax.axis_size("tp")
+    rows, width = tokens.shape
+    n_exp, hid, features = w_gate.shape
+    units, out_part = w_down.shape[1], w_down.shape[2]
+    n_z = n_tp // CORES
+    n_tok = rows * n_ep
+    n_send = (n_z - 1) + n_ep + (n_ep - 1) + (n_z - 1) * n_ep + n_z * (n_ep - 1)
+    n_send += 2 * (n_z - 1) + 1 + (n_ep - 1) + (n_tp - 1)
+    vmem = pl.BlockSpec(memory_space=pltpu.VMEM)
+    hbm = pl.BlockSpec(memory_space=pl.ANY)
+    dma = pltpu.SemaphoreType.DMA
+    return pl.pallas_call(
+        functools.partial(dense_kernel, n_ep, n_tp),
+        out_shape=jax.ShapeDtypeStruct((rows, out_part), jnp.bfloat16),
+        in_specs=[hbm, vmem, vmem, hbm, hbm, hbm, vmem],
+        out_specs=vmem,
+        scratch_shapes=[
+            pltpu.VMEM((n_tp, n_tok, width), jnp.bfloat16),
+            pltpu.VMEM((n_tok, LANES), jnp.float32),
+            pltpu.VMEM((2 * n_exp, hid, features), jnp.bfloat16),
+            pltpu.VMEM((n_exp, units, out_part), jnp.bfloat16),
+            pltpu.VMEM((n_tok, max(out_part, 2 * n_exp * hid)), jnp.float32),
+            pltpu.VMEM((n_tp, n_tok, n_exp * hid), jnp.bfloat16),
+            pltpu.VMEM((n_ep, rows, out_part), jnp.bfloat16),
+            pltpu.VMEM((n_ep, rows, out_part), jnp.bfloat16),
+            pltpu.VMEM((1, LANES), jnp.float32),
+            pltpu.VMEM((n_tp, 1, LANES), jnp.float32),
+            dma((4,)),
+            dma((n_send,)),
+            dma((n_ep, n_tp)),
+            dma((n_ep,)),
+            dma((n_tp,)),
+            dma((n_ep,)),
+            dma((n_tp,)),
+        ],
+        compiler_params=pltpu.CompilerParams(collective_id=0, has_side_effects=True),
+    )(tokens, routing, gate_weights, w_gate, w_up, w_down, out_gain.reshape(1, -1))
+
+
+def body(tokens, routing, gate_weights, w_gate, w_up, w_down, out_gain):
+    slots = 2 * tokens.shape[0] * TOPK // (EXP_DEV * lax.axis_size("ep"))
+    step = dense_body if slots >= tokens.shape[0] else routed_body
+    return step(tokens, routing, gate_weights, w_gate, w_up, w_down, out_gain)
+
+
 def solution(mesh):
     placed = (
         P("ep", "tp"),

time: 103 us -> 39.2 us (0.38)
  blocking collectives: 38.2 us -> 0 us
  Pallas kernels: 0 us -> 34.8 us
  waiting for transfers between devices: 34.7 us -> 0 us
  between operations: 13.5 us -> 0.01 us
  matrix products: 4.63 us -> 0 us
  other arithmetic: 3.86 us -> 0 us
  starting transfers between devices: 3.65 us -> 0 us
    pallas_call x0 -> x1, Pallas kernels: none -> 34.8 us  [dense_body(): pl.pallas_call(functools.partial(dense_kernel, n_ep, n_tp), out_shape=jax...]
    all_gather x1 -> x0, waiting for transfers between devices: 28.9 us -> none  [body(): piece_cols = lax.all_gather(arrived, 'tp', axis=2, tiled=True)]
    all_gather x1 -> x0, blocking collectives: 13.9 us -> none  [body(): lax.all_gather(hidden, 'tp', axis=1, tiled=True)]
    psum x1 -> x0, blocking collectives: 13.6 us -> none  [body(): square_total = lax.psum(jnp.sum(combined * combined, axis=1), 'tp')]
    all_to_all x1 -> x0, blocking collectives: 10.7 us -> none  [body(): lax.all_to_all(outgoing, 'ep', split_axis=1, concat_axis=1, tiled=True)]
    all_to_all x1 -> x0, waiting for transfers between devices: 5.77 us -> none  [body(): lax.all_to_all(expert_out.reshape(EXP_DEV, ep_count, slot_count, out_part...]
    dot_general x4 -> x0, matrix products: 4.63 us -> none  [the longest x1 2.45 us: body(): jnp.einsum('efn,esn->efs', w_gate, piece_cols, preferred_element_type=jnp...]
    all_to_all x1 -> x0, starting transfers between devices: 3.65 us -> none  [body(): lax.all_to_all(expert_out.reshape(EXP_DEV, ep_count, slot_count, out_part...]
  transfers between devices with their start and end apart: 2 -> 0, of which waited for: 2 -> 0; matrix products, arithmetic and copies ran while one was open for 0% -> 0% of each run, Pallas kernels for 0% -> 0%
where the time goes in v1:
time: 39.2 us; the launch traced here: 38.9 us
  Pallas kernels  34.8 us (89%)
  local copies, waits for them, and re-layouts  4.1 us (10%)
    pallas_call x1, Pallas kernels, dense_body(): pl.pallas_call(functools.partial(dense_kernel, n_ep, n_tp), out_shape=jax...  34.8 us
    unnamed x3, local copies, waits for them, and re-layouts  4.1 us

profile of v1, /device:TPU:0, one launch (start us, length us, event | category | flops | bytes accessed | tf_op | source)
XLA Modules:
  0.0 38.9 jit_solution(10557233164577271441)
XLA Ops:
  0.0 1.4 %copy.8.route_ref = s32[32,4]{1,0:T(8,128)} copy(s32[32,4]{0,1:T(4,128)} %param.8) | data formatting | bytes 1024 | tf_op args[1]
  1.4 1.4 %copy.9.gates_ref = f32[32,4]{1,0:T(8,128)} copy(f32[32,4]{0,1:T(4,128)} %param.9) | data formatting | bytes 1024 | tf_op args[2]
  2.7 34.8 %shard_map.73 = bf16[32,512]{1,0:T(8,128)(2,1)} custom-call(bf16[32,512]{1,0:T(8,128)(2,1)} %tok_hbm.1, s32[32,4]{1,0:T(8,128)} %copy.8.route_ref, f32[32,4]{1,0:T(8,128)} %copy.9.gates_ref, bf16[2,128,4096]{2,1,0:T(8,128)(2,1)} %wg_hbm.1, bf16[2,128,4096]{2,1,0:T(8,128)(2,1)} %wu_hbm.1, bf16[2,1024,512]{2,1,0:T(8,128)(2,1)} %wd_hbm.1, f32[1,512]{1,0:T(1,128)} %bitcast.1), custom_call_target="tpu_custom_call" | custom-call | tf_op jit(solution)/shard_map/pallas_call | solution.py:314
  37.5 1.4 %copy.11 = bf16[32,512]{1,0:T(8,128)(2,1)} copy(bf16[32,512]{1,0:T(8,128)(2,1)} %shard_map.73) | data formatting | bytes 65536

commit v2 on v1

--- a/solution.py
+++ b/solution.py
@@ -91,7 +91,6 @@
     g_all,
     w_v,
     wd_v,
-    acc,
     h_all,
     p_send,
     p_recv,
@@ -112,14 +111,18 @@
     c = t % CORES
     mate = z * CORES + (1 - c)
     rows, width = tok_hbm.shape
-    tokens = rows * n_ep
     n_exp, hid = wg_hbm.shape[0], wg_hbm.shape[1]
     features = wg_hbm.shape[2]
     mine = pl.ds(pl.multiple_of(e * rows, rows), rows)
 
     barrier = pltpu.get_barrier_semaphore()
     tp_peers = [lax.rem(t + d, n_tp) for d in range(1, n_tp)]
-    ep_peers = [lax.rem(e + d, n_ep) for d in range(1, n_ep)]
+    ep_list = []
+    for d in range(n_ep):
+        far = lax.rem(e + 2 * (d // 2), n_ep)
+        ep_list.append(far + 1 - 2 * lax.rem(far, 2) if d % 2 else far)
+    ep_peers = ep_list[1:]
+    groups = [ep_list[:1], ep_list[1:-1], ep_list[-1:]]
     z_order = [0]
     for d in range(1, n_z // 2 + 1):
         z_order += [d] if 2 * d == n_z else [d, n_z - d]
@@ -138,11 +141,13 @@
     wd_copy = pltpu.make_async_copy(wd_hbm, wd_v, loc_sem.at[3])
     wd_copy.start()
 
+    expert = lax.broadcasted_iota(jnp.int32, (n_ep * n_exp, rows), 0)
+    table = jnp.zeros((n_ep * n_exp, rows), jnp.float32)
+    for k in range(route_ref.shape[0]):
+        table += jnp.where(route_ref[k : k + 1, :] == expert, gates_ref[k : k + 1, :], 0.0)
+    g_all[e, :, 0:rows] = table
     lane = lax.broadcasted_iota(jnp.int32, (rows, LANES), 1)
-    table = jnp.zeros((rows, LANES), jnp.float32)
-    for k in range(route_ref.shape[1]):
-        table += jnp.where(route_ref[:, k : k + 1] == lane, gates_ref[:, k : k + 1], 0.0)
-    g_all[mine, :] = table
+    eye = lax.broadcasted_iota(jnp.int32, (rows, LANES), 0) == lane
 
     sends = []
 
@@ -183,7 +188,7 @@
         send_x(e, t, (peer, t))
     send_x(e, t, (e, mate))
     for peer in ep_peers:
-        send(g_all.at[mine, :], g_all.at[mine, :], g_sem.at[e], (peer, t))
+        send(g_all.at[e], g_all.at[e], g_sem.at[e], (peer, t))
     for zz in z_list[1:]:
         tp = zz * CORES + c
         arrive(x_block(e, tp), x_sem.at[e, tp])
@@ -193,98 +198,124 @@
     wg_copy.wait()
     wu_copy.wait()
 
-    square = jnp.zeros((tokens, LANES), jnp.float32)
-
-    def up_part(tp, first, square):
-        x = x_all[tp]
+
+    def rows_of(ep):
+        return pl.ds(pl.multiple_of(ep * rows, rows), rows)
+
+    def stack(pieces):
+        return pieces[0] if len(pieces) == 1 else jnp.concatenate(pieces, axis=0)
+
+    def up_part(group, tp, state):
+        x = stack([x_all[tp, rows_of(ep), :] for ep in group])
         cols = pl.ds(pl.multiple_of(tp * width, width), width)
         w = w_v[:, :, cols].reshape(2 * n_exp * hid, width)
         part = lax.dot_general(
             x, w, (((1,), (1,)), ((), ())), preferred_element_type=jnp.float32
         )
-        if first:
-            acc[...] = part
-        else:
-            acc[...] += part
+        square = jnp.zeros((x.shape[0], LANES), jnp.float32) if state is None else state[1]
         for i in range(width // LANES):
             piece = x[:, i * LANES : (i + 1) * LANES].astype(jnp.float32)
             square = square + piece * piece
-        return square
-
-    for i, zz in enumerate(z_list):
-        tp = zz * CORES + c
-        for peer in ep_peers:
-            arrive(x_block(peer, tp), x_sem.at[peer, tp])
-            send_x(peer, tp, (e, mate))
-        square = up_part(tp, i == 0, square)
-    for zz in z_list:
-        tp = zz * CORES + 1 - c
-        for ep in [e] + ep_peers:
-            arrive(x_block(ep, tp), x_sem.at[ep, tp])
-        square = up_part(tp, False, square)
-    for peer in ep_peers:
-        theirs = g_all.at[pl.ds(pl.multiple_of(peer * rows, rows), rows), :]
-        arrive(theirs, g_sem.at[peer])
-
-    scale = lax.rsqrt(jnp.sum(square, axis=1, keepdims=True) / features + norm_eps)
-    every_lane = lax.broadcasted_iota(jnp.int32, (tokens, LANES), 1)
-    for j in range(n_exp):
-        gate = acc[:, j * hid : (j + 1) * hid] * scale
-        up = acc[:, (n_exp + j) * hid : (n_exp + j + 1) * hid] * scale
-        weight = jnp.sum(
-            jnp.where(every_lane == e * n_exp + j, g_all[...], 0.0), axis=1, keepdims=True
-        )
-        h_all[t, :, j * hid : (j + 1) * hid] = (
-            gate / (1.0 + jnp.exp(-gate)) * up * weight
-        ).astype(jnp.bfloat16)
-
-    def send_h(tp, device):
-        send(h_all.at[tp], h_all.at[tp], h_sem.at[tp], device)
-
-    for zz in z_list[1:]:
-        send_h(t, (e, zz * CORES + c))
-    send_h(t, (e, mate))
+        return (part if state is None else state[0] + part), square
+
+    def h_block(ep, tp):
+        return h_all.at[tp, rows_of(ep), :]
+
+    def send_h(ep, tp, device):
+        send(h_block(ep, tp), h_block(ep, tp), h_sem.at[ep, tp], device)
+
+    def finish_hidden(group, state):
+        total, square = state
+        scale = lax.rsqrt(jnp.sum(square, axis=1, keepdims=True) / features + norm_eps)
+        for j in range(n_exp):
+            weight = stack(
+                [
+                    jnp.sum(
+                        jnp.where(eye, g_all[ep, pl.ds(e * n_exp + j, 1), :], 0.0),
+                        axis=1,
+                        keepdims=True,
+                    )
+                    for ep in group
+                ]
+            )
+            gate = total[:, j * hid : (j + 1) * hid] * scale
+            up = total[:, (n_exp + j) * hid : (n_exp + j + 1) * hid] * scale
+            part = (gate / (1.0 + jnp.exp(-gate)) * up * weight).astype(jnp.bfloat16)
+            for i, ep in enumerate(group):
+                h_all[t, rows_of(ep), j * hid : (j + 1) * hid] = part[i * rows : (i + 1) * rows]
+        for ep in group:
+            for zz in z_list[1:]:
+                send_h(ep, t, (e, zz * CORES + c))
+            send_h(ep, t, (e, mate))
+
+    def relay_h(group):
+        for zz in z_list[1:]:
+            tp = zz * CORES + c
+            for ep in group:
+                arrive(h_block(ep, tp), h_sem.at[ep, tp])
+                send_h(ep, tp, (e, mate))
+
+    def down(group):
+        for zz in z_list:
+            tp = zz * CORES + 1 - c
+            for ep in group:
+                arrive(h_block(ep, tp), h_sem.at[ep, tp])
+        total = None
+        for tp in range(n_tp):
+            h = stack([h_all[tp, rows_of(ep), :] for ep in group])
+            for j in range(n_exp):
+                part = jnp.dot(
+                    h[:, j * hid : (j + 1) * hid],
+                    wd_v[j, tp * hid : (tp + 1) * hid, :],
+                    preferred_element_type=jnp.float32,
+                )
+                total = part if total is None else total + part
+        return total
+
+    def own_side(group, first):
+        state = None
+        for zz in z_list:
+            tp = zz * CORES + c
+            if not first:
+                for ep in group:
+                    arrive(x_block(ep, tp), x_sem.at[ep, tp])
+                    send_x(ep, tp, (e, mate))
+            state = up_part(group, tp, state)
+        return state
+
+    def mate_side(group, state):
+        for zz in z_list:
+            tp = zz * CORES + 1 - c
+            for ep in group:
+                arrive(x_block(ep, tp), x_sem.at[ep, tp])
+            state = up_part(group, tp, state)
+        return state
+
+    near, middle, last = groups
+    finish_hidden(near, mate_side(near, own_side(near, True)))
+    for peer in ep_peers:
+        arrive(g_all.at[peer], g_sem.at[peer])
+    finish_hidden(middle, mate_side(middle, own_side(middle, False)))
+    relay_h(near)
+    finish_hidden(last, mate_side(last, own_side(last, False)))
     wd_copy.wait()
-
-    def down_part(tp, first):
-        part = None
-        for j in range(n_exp):
-            units = pl.ds(pl.multiple_of(tp * hid, hid), hid)
-            one = jnp.dot(
-                h_all[tp, :, j * hid : (j + 1) * hid],
-                wd_v[j, units, :],
-                preferred_element_type=jnp.float32,
-            )
-            part = one if part is None else part + one
-        if first:
-            acc[...] = part
-        else:
-            acc[...] += part
-
-    down_part(t, True)
-    arrive(h_all.at[mate], h_sem.at[mate])
-    down_part(mate, False)
-    for zz in z_list[1:]:
-        tp = zz * CORES + c
-        arrive(h_all.at[tp], h_sem.at[tp])
-        send_h(tp, (e, mate))
-        down_part(tp, False)
-    for zz in z_list[1:]:
-        tp = zz * CORES + 1 - c
-        arrive(h_all.at[tp], h_sem.at[tp])
-        down_part(tp, False)
-
-    for peer in ep_peers:
-        theirs = pl.ds(pl.multiple_of(peer * rows, rows), rows)
-        p_send[peer] = acc[theirs, :].astype(jnp.bfloat16)
-        send(p_send.at[peer], p_recv.at[e], p_sem.at[e], (peer, t))
-    combined = acc[mine, :]
+    combined = down(near)
+    relay_h(middle)
+
+    def give_back(group):
+        total = down(group)
+        for i, peer in enumerate(group):
+            p_send[peer] = total[i * rows : (i + 1) * rows, :].astype(jnp.bfloat16)
+            send(p_send.at[peer], p_recv.at[e], p_sem.at[e], (peer, t))
+
+    give_back(middle)
+    relay_h(last)
+    give_back(last)
     for peer in ep_peers:
         arrive(p_recv.at[peer], p_sem.at[peer])
         combined = combined + p_recv[peer].astype(jnp.float32)
 
     column = jnp.sum(combined * combined, axis=1, keepdims=True)
-    eye = lax.broadcasted_iota(jnp.int32, (rows, LANES), 0) == lane
     s_send[...] = jnp.sum(jnp.where(eye, column, 0.0), axis=0, keepdims=True)
     for peer in tp_peers:
         send(s_send, s_all.at[t], s_sem.at[t], (e, peer))
@@ -304,24 +335,21 @@
     rows, width = tokens.shape
     n_exp, hid, features = w_gate.shape
     units, out_part = w_down.shape[1], w_down.shape[2]
-    n_z = n_tp // CORES
     n_tok = rows * n_ep
-    n_send = (n_z - 1) + n_ep + (n_ep - 1) + (n_z - 1) * n_ep + n_z * (n_ep - 1)
-    n_send += 2 * (n_z - 1) + 1 + (n_ep - 1) + (n_tp - 1)
+    n_send = 2 * n_ep * n_tp + 2 * n_ep + n_tp
     vmem = pl.BlockSpec(memory_space=pltpu.VMEM)
     hbm = pl.BlockSpec(memory_space=pl.ANY)
     dma = pltpu.SemaphoreType.DMA
     return pl.pallas_call(
         functools.partial(dense_kernel, n_ep, n_tp),
-        out_shape=jax.ShapeDtypeStruct((rows, out_part), jnp.bfloat16),
+        out_shape=pltpu.VMEM((rows, out_part), jnp.bfloat16),
         in_specs=[hbm, vmem, vmem, hbm, hbm, hbm, vmem],
         out_specs=vmem,
         scratch_shapes=[
             pltpu.VMEM((n_tp, n_tok, width), jnp.bfloat16),
-            pltpu.VMEM((n_tok, LANES), jnp.float32),
+            pltpu.VMEM((n_ep, n_ep * n_exp, LANES), jnp.float32),
             pltpu.VMEM((2 * n_exp, hid, features), jnp.bfloat16),
             pltpu.VMEM((n_exp, units, out_part), jnp.bfloat16),
-            pltpu.VMEM((n_tok, max(out_part, 2 * n_exp * hid)), jnp.float32),
             pltpu.VMEM((n_tp, n_tok, n_exp * hid), jnp.bfloat16),
             pltpu.VMEM((n_ep, rows, out_part), jnp.bfloat16),
             pltpu.VMEM((n_ep, rows, out_part), jnp.bfloat16),
@@ -331,12 +359,12 @@
             dma((n_send,)),
             dma((n_ep, n_tp)),
             dma((n_ep,)),
-            dma((n_tp,)),
+            dma((n_ep, n_tp)),
             dma((n_ep,)),
             dma((n_tp,)),
         ],
         compiler_params=pltpu.CompilerParams(collective_id=0, has_side_effects=True),
-    )(tokens, routing, gate_weights, w_gate, w_up, w_down, out_gain.reshape(1, -1))
+    )(tokens, routing.T, gate_weights.T, w_gate, w_up, w_down, out_gain.reshape(1, -1))
 
 
 def body(tokens, routing, gate_weights, w_gate, w_up, w_down, out_gain):

time: 39.2 us -> 33.5 us (0.85)
  local copies, waits for them, and re-layouts: 4.1 us -> 0.62 us
  Pallas kernels: 34.8 us -> 32.7 us
    unnamed x3 -> x1, local copies, waits for them, and re-layouts: 4.1 us -> 0.62 us
    pallas_call x1, Pallas kernels: 34.8 us -> 32.7 us  [dense_body(): pl.pallas_call(functools.partial(dense_kernel, n_ep, n_tp), out_shape=plt...]
where the time goes in v2:
time: 33.5 us; the launch traced here: 33.3 us
  Pallas kernels  32.7 us (98%)
  local copies, waits for them, and re-layouts  0.62 us (2%)
    pallas_call x1, Pallas kernels, dense_body(): pl.pallas_call(functools.partial(dense_kernel, n_ep, n_tp), out_shape=plt...  32.7 us

profile of v2, /device:TPU:0, one launch (start us, length us, event | category | flops | bytes accessed | tf_op | source)
XLA Modules:
  0.0 33.3 jit_solution(2374068609490838331)
XLA Ops:
  0.0 32.7 %shard_map.73 = bf16[32,512]{1,0:T(8,128)(2,1)S(1)} custom-call(bf16[32,512]{1,0:T(8,128)(2,1)} %tok_hbm.1, s32[4,32]{1,0:T(4,128)} %bitcast.3, f32[4,32]{1,0:T(4,128)} %bitcast.4, bf16[2,128,4096]{2,1,0:T(8,128)(2,1)} %wg_hbm.1, bf16[2,128,4096]{2,1,0:T(8,128)(2,1)} %wu_hbm.1, bf16[2,1024,512]{2,1,0:T(8,128)(2,1)} %wd_hbm.1, f32[1,512]{1,0:T(1,128)} %bitcast.5), custom_call_target="tpu_custom_call" | custom-call | tf_op jit(solution)/shard_map/pallas_call | solution.py:343
  32.7 0.6 %copy.9 = bf16[32,512]{1,0:T(8,128)(2,1)} copy(bf16[32,512]{1,0:T(8,128)(2,1)S(1)} %shard_map.73) | data formatting | bytes 65536

commit v3 on v2

--- a/solution.py
+++ b/solution.py
@@ -123,10 +123,11 @@
         ep_list.append(far + 1 - 2 * lax.rem(far, 2) if d % 2 else far)
     ep_peers = ep_list[1:]
     groups = [ep_list[:1], ep_list[1:-1], ep_list[-1:]]
-    z_order = [0]
-    for d in range(1, n_z // 2 + 1):
-        z_order += [d] if 2 * d == n_z else [d, n_z - d]
+    z_order = range(n_z)
     z_list = [lax.rem(z + d, n_z) for d in z_order]
+    z_give = [lax.rem(z + n_z - d, n_z) for d in z_order[1:]]
+    h_list = [z] + [lax.rem(z + d, n_z) for d in z_order[1:]]
+    h_give = [lax.rem(z + n_z - d, n_z) for d in z_order[1:]]
     for peer in tp_peers:
         pl.semaphore_signal(barrier, inc=1, device_id=(e, peer), device_id_type=MESH)
     for peer in ep_peers:
@@ -182,7 +183,7 @@
     tok_copy.wait()
     pl.semaphore_wait(barrier, n_tp - 1 + n_ep - 1)
 
-    for zz in z_list[1:]:
+    for zz in z_give:
         send_x(e, t, (e, zz * CORES + c))
     for peer in ep_peers:
         send_x(e, t, (peer, t))
@@ -244,19 +245,19 @@
             for i, ep in enumerate(group):
                 h_all[t, rows_of(ep), j * hid : (j + 1) * hid] = part[i * rows : (i + 1) * rows]
         for ep in group:
-            for zz in z_list[1:]:
+            for zz in h_give:
                 send_h(ep, t, (e, zz * CORES + c))
             send_h(ep, t, (e, mate))
 
     def relay_h(group):
-        for zz in z_list[1:]:
+        for zz in h_list[1:]:
             tp = zz * CORES + c
             for ep in group:
                 arrive(h_block(ep, tp), h_sem.at[ep, tp])
                 send_h(ep, tp, (e, mate))
 
     def down(group):
-        for zz in z_list:
+        for zz in h_list:
             tp = zz * CORES + 1 - c
             for ep in group:
                 arrive(h_block(ep, tp), h_sem.at[ep, tp])

time: 33.5 us -> 33 us (0.985)
  Pallas kernels: 32.7 us -> 32.1 us
    pallas_call x1, Pallas kernels: 32.7 us -> 32.1 us  [dense_body(): pl.pallas_call(functools.partial(dense_kernel, n_ep, n_tp), out_shape=plt...]
where the time goes in v3:
time: 33 us; the launch traced here: 32.8 us
  Pallas kernels  32.1 us (97%)
  local copies, waits for them, and re-layouts  0.62 us (2%)
    pallas_call x1, Pallas kernels, dense_body(): pl.pallas_call(functools.partial(dense_kernel, n_ep, n_tp), out_shape=plt...  32.1 us

profile of v3, /device:TPU:0, one launch (start us, length us, event | category | flops | bytes accessed | tf_op | source)
XLA Modules:
  0.0 32.8 jit_solution(16736297019863097258)
XLA Ops:
  0.0 32.1 %shard_map.73 = bf16[32,512]{1,0:T(8,128)(2,1)S(1)} custom-call(bf16[32,512]{1,0:T(8,128)(2,1)} %tok_hbm.1, s32[4,32]{1,0:T(4,128)} %bitcast.3, f32[4,32]{1,0:T(4,128)} %bitcast.4, bf16[2,128,4096]{2,1,0:T(8,128)(2,1)} %wg_hbm.1, bf16[2,128,4096]{2,1,0:T(8,128)(2,1)} %wu_hbm.1, bf16[2,1024,512]{2,1,0:T(8,128)(2,1)} %wd_hbm.1, f32[1,512]{1,0:T(1,128)} %bitcast.5), custom_call_target="tpu_custom_call" | custom-call | tf_op jit(solution)/shard_map/pallas_call | solution.py:344
  32.1 0.6 %copy.9 = bf16[32,512]{1,0:T(8,128)(2,1)} copy(bf16[32,512]{1,0:T(8,128)(2,1)S(1)} %shard_map.73) | data formatting | bytes 65536
